TPU v7x, 32 devices: a whole 2x2x4 slice. The times are simulated.
32 devices in a mesh: fs: 16 (over z, y, x), tp: 2 (over core).
Axes of the slice: x: 2, y: 2, z: 4, core: 2. Of those that a mesh axis runs over, the one named last changes fastest.
Arguments:
- tokens: bfloat16 [3072, 2048], P('fs'), may hold values from -6 to 6
- route_ids: int32 [3072, 2], P('fs'), may hold values from 0 to 7, all different within a row; in each aligned block of 192 rows (0 to 191, 192 to 383, ...) at most 96 rows name the same one
- route_logits: float32 [3072, 2], P('fs'), may hold values from -6 to 6
- norm_gain: float32 [2048], P('fs'), may hold values from 0.1 to 1.9
- gate_weight: float32 [8, 2048, 2048], P(None, 'fs', 'tp'), may hold values from -0.125 to 0.125
- up_weight: float32 [8, 2048, 2048], P(None, 'fs', 'tp'), may hold values from -0.125 to 0.125
- down_weight: float32 [8, 2048, 2048], P(None, 'fs', 'tp'), may hold values from -0.125 to 0.125
Outputs:
- mixed: bfloat16 [3072, 2048], P('fs')
- gate_copies: bfloat16 [16, 2048, 2048], P('fs', None, 'tp')
- up_copies: bfloat16 [16, 2048, 2048], P('fs', None, 'tp')
- down_copies: bfloat16 [16, 2048, 2048], P('fs', None, 'tp')
Inputs may be any that keep to these rules, and one draw needn't show every extreme that they name: `route_ids`: each row names 2 different experts. Among the rows of one index of fs no expert is named by more than 96 rows, a bound that some of them reach.
All inputs are finite; a program needn't handle non-finite values.
Results may differ from a plain program's by a relative error of at most 0.014.
Values may be sent and summed in bfloat16 or wider, within the bound.
A program may use at most 128 MiB of HBM per device.

v0:
```python
import jax
import jax.numpy as jnp
from jax import lax
from jax.sharding import PartitionSpec as P

CAP = 96


def body(tokens, route_ids, route_logits, norm_gain, gate_weight, up_weight, down_weight):
    experts = gate_weight.shape[0]
    fs_count = lax.axis_size("fs")
    copies = fs_count // experts
    per_peer = CAP // copies
    tok_rows = tokens.shape[0]
    width = tokens.shape[1]
    scaled_gain = norm_gain[None, :, None]
    gate_send = jnp.repeat((scaled_gain * gate_weight).astype(jnp.bfloat16), copies, axis=0)
    up_send = jnp.repeat((scaled_gain * up_weight).astype(jnp.bfloat16), copies, axis=0)
    down_send = jnp.repeat(down_weight.astype(jnp.bfloat16), copies, axis=0)
    gate_new, up_new, down_new = (
        lax.all_to_all(gate_send, "fs", split_axis=0, concat_axis=1, tiled=True),
        lax.all_to_all(up_send, "fs", split_axis=0, concat_axis=1, tiled=True),
        lax.all_to_all(down_send, "fs", split_axis=0, concat_axis=1, tiled=True),
    )
    values = tokens.astype(jnp.float32)
    center = jnp.mean(values, axis=1, keepdims=True)
    spread = jnp.mean(jnp.square(values - center), axis=1, keepdims=True)
    normed = ((values - center) * lax.rsqrt(spread + 1e-06)).astype(jnp.bfloat16)
    flat_ids = route_ids.reshape(-1)
    onehot_table = (flat_ids[:, None] == jnp.arange(experts, dtype=jnp.int32)[None, :]).astype(
        jnp.int32
    )
    before = jnp.cumsum(onehot_table, axis=0) - onehot_table
    order_rank = jnp.sum(before * onehot_table, axis=1)
    dest_flat = (flat_ids * copies + order_rank % copies) * per_peer + order_rank // copies
    owners = jnp.arange(flat_ids.shape[0], dtype=jnp.int32) // route_ids.shape[1]
    slot_token = jnp.full((experts * CAP,), tok_rows, jnp.int32).at[dest_flat].set(owners)
    padded = jnp.concatenate([normed, jnp.zeros((1, width), jnp.bfloat16)], axis=0)
    send_rows = padded[slot_token].reshape(fs_count, per_peer, width)
    gate_matrix = gate_new[0]
    up_matrix = up_new[0]
    col_count = width // lax.axis_size("tp")
    col_start = lax.axis_index("tp") * col_count
    own_cols = lax.dynamic_slice_in_dim(send_rows, col_start, col_count, 2)
    arrived = lax.all_to_all(own_cols, "fs", split_axis=0, concat_axis=0, tiled=True).reshape(
        -1, col_count
    )
    piece = lax.all_gather(arrived, "tp", axis=1, tiled=True)
    gate_act = jnp.dot(piece, gate_matrix, preferred_element_type=jnp.float32)
    up_act = jnp.dot(piece, up_matrix, preferred_element_type=jnp.float32)
    hidden = (jax.nn.silu(gate_act) * up_act).astype(jnp.bfloat16)
    partial_value = jnp.einsum("rf,df->rd", hidden, down_new[0], preferred_element_type=jnp.float32)
    share = lax.psum_scatter(
        partial_value.astype(jnp.bfloat16), "tp", scatter_dimension=1, tiled=True
    )
    back_part = lax.all_to_all(
        share.reshape(fs_count, per_peer, col_count), "fs", split_axis=0, concat_axis=0, tiled=True
    )
    returned = lax.all_gather(back_part, "tp", axis=2, tiled=True).reshape(-1, width)
    picked = returned[dest_flat].reshape(tok_rows, route_ids.shape[1], width).astype(jnp.float32)
    first_weight = jax.nn.sigmoid(route_logits[:, 0] - route_logits[:, 1])
    second_weight = jax.nn.sigmoid(route_logits[:, 1] - route_logits[:, 0])
    mixed = (first_weight[:, None] * picked[:, 0] + second_weight[:, None] * picked[:, 1]).astype(
        jnp.bfloat16
    )
    return (mixed, gate_new, up_new, down_new)


def solution(mesh):
    return jax.shard_map(
        body,
        mesh=mesh,
        in_specs=(
            P("fs", None),
            P("fs", None),
            P("fs", None),
            P("fs"),
            P(None, "fs", "tp"),
            P(None, "fs", "tp"),
            P(None, "fs", "tp"),
        ),
        out_specs=(P("fs", None), P("fs", None, "tp"), P("fs", None, "tp"), P("fs", None, "tp")),
        check_vma=False,
    )
```

profile of v0, /device:TPU:0, one launch (start us, length us, event | category | flops | bytes accessed | tf_op | source)
XLA Modules:
  0.0 482.2 jit_solution(4758031760930865264)
XLA Ops:
  10.5 2.9 scatter_custom_fusion
  18.0 4.2 gather_fusion
  22.2 2.7 constant_dynamic-slice_fusion
  24.9 8.4 %all-to-all-start = ((bf16[16,48,1024]{2,1,0:T(8,128)(2,1)}), bf16[16,48,1024]{2,1,0:T(8,128)(2,1)}, u32[]{:S(2)}, u32[]{:S(2)}) async-start(bf16[16,48,1024]{2,1,0:T(8,128)(2,1)} %constant_dynamic-slice_fusion), calls=%async_computation | async-start | bytes 3145728 | tf_op jit(solution)/shard_map/all_to_all | solution.py:45
  33.3 6.1 %multiply_convert_fusion = (bf16[8,128,1024]{2,1,0:T(8,128)(2,1)S(1)}, bf16[8,128,1024]{2,1,0:T(8,128)(2,1)}) fusion(f32[8,128,1024]{2,1,0:T(8,128)} %param.12, f32[128]{0:T(128)S(1)} %copy-done.2, f32[8,128,1024]{2,1,0:T(8,128)} %param.11), kind=kLoop, calls=%fused_computation.3 | loop fusion | flops 4194304 | bytes 12583424 | tf_op jit(solution)/shard_map/convert_element_type | solution.py:18
  39.4 28.0 %all-to-all-done = bf16[16,48,1024]{2,1,0:T(8,128)(2,1)} async-done(((bf16[16,48,1024]{2,1,0:T(8,128)(2,1)}), bf16[16,48,1024]{2,1,0:T(8,128)(2,1)}, u32[]{:S(2)}, u32[]{:S(2)}) %all-to-all-start) | async-done | bytes 1572896 | tf_op jit(solution)/shard_map/all_to_all | solution.py:45
  69.6 100.9 %all_to_all.46 = bf16[16,128,1024]{2,1,0:T(8,128)(2,1)} all-to-all(bf16[16,128,1024]{2,1,0:T(8,128)(2,1)S(1)} %bitcast.48), channel_id=1, replica_groups=mesh['fs'=16,'tp'=2] {'fs'}, dimensions={0} | all-to-all | bytes 8388608 | tf_op jit(solution)/shard_map/all_to_all | solution.py:21
  170.5 2.6 broadcast_in_dim.13
  173.1 4.5 all-to-all-start.2
  177.6 2.5 convert_element_type.44
  180.2 75.9 %all-to-all-done.2 = bf16[16,128,1024]{2,1,0:T(8,128)(2,1)} async-done(((bf16[16,128,1024]{2,1,0:T(8,128)(2,1)}), bf16[16,128,1024]{2,1,0:T(8,128)(2,1)}, u32[]{:S(2)}, u32[]{:S(2)}) %all-to-all-start.2) | async-done | bytes 4194336 | tf_op jit(solution)/shard_map/all_to_all | solution.py:22
  256.1 2.6 broadcast_in_dim.28
  258.7 18.6 %all-to-all-start.3 = ((bf16[16,128,1024]{2,1,0:T(8,128)(2,1)}), bf16[16,128,1024]{2,1,0:T(8,128)(2,1)}, u32[]{:S(2)}, u32[]{:S(2)}) async-start(bf16[16,128,1024]{2,1,0:T(8,128)(2,1)} %bitcast.46), calls=%async_computation.3 | async-start | bytes 8388608 | tf_op jit(solution)/shard_map/all_to_all | solution.py:23
  278.2 14.8 %all-gather.3.cloned.1.call-done = bf16[768,2048]{1,0:T(8,128)(2,1)} async-done(((bf16[768,1024]{1,0:T(8,128)(2,1)}), bf16[768,2048]{1,0:T(8,128)(2,1)}) %all-gather.3.cloned.1.call-update) | async-done | bytes 3145744 | tf_op jit(solution)/shard_map/all_gather | solution.py:48
  293.0 8.2 %fusion.20 = f32[768,1024]{1,0:T(8,128)} fusion(bf16[768,2048]{1,0:T(8,128)(2,1)} %all-gather.3.cloned.1.call-done, bf16[2048,1024]{1,0:T(8,128)(2,1)} %bitcast.44), kind=kOutput, calls=%fused_computation.54 | convolution fusion | flops 3221225472 | bytes 10485760 | tf_op jit(solution)/shard_map/dot_general | solution.py:49
  301.2 54.5 %all-to-all-done.3 = bf16[16,128,1024]{2,1,0:T(8,128)(2,1)} async-done(((bf16[16,128,1024]{2,1,0:T(8,128)(2,1)}), bf16[16,128,1024]{2,1,0:T(8,128)(2,1)}, u32[]{:S(2)}, u32[]{:S(2)}) %all-to-all-start.3) | async-done | bytes 4194336 | tf_op jit(solution)/shard_map/all_to_all | solution.py:23
  355.7 12.5 %convolution_convert_fusion = bf16[768,2048]{1,0:T(8,128)(2,1)} fusion(bf16[2048,1024]{1,0:T(8,128)(2,1)} %bitcast.10, f32[768,1024]{1,0:T(8,128)} %fusion.20, bf16[768,2048]{1,0:T(8,128)(2,1)} %all-gather.3.cloned.1.call-done, bf16[2048,1024]{1,0:T(8,128)(2,1)} %bitcast.8), kind=kOutput, calls=%fused_computation.5 | convolution fusion | flops 6448742400 | bytes 17825792 | tf_op jit(solution)/shard_map/rf,df->rd/dot_general | solution.py:52
  368.4 24.9 %reduce-scatter.2.cloned.1.call-done = bf16[768,1024]{1,0:T(8,128)(2,1)} async-done(((bf16[768,2048]{1,0:T(8,128)(2,1)}), bf16[768,1024]{1,0:T(8,128)(2,1)}) %reduce-scatter.2.cloned.1.call-update) | async-done | bytes 1572880 | tf_op jit(solution)/shard_map/reduce_scatter | solution.py:53
  393.2 44.9 %all_to_all.47 = bf16[16,48,1024]{2,1,0:T(8,128)(2,1)} all-to-all(bf16[16,48,1024]{2,1,0:T(8,128)(2,1)} %bitcast.50), channel_id=1, replica_groups=mesh['fs'=16,'tp'=2] {'fs'}, dimensions={0} | all-to-all | bytes 3145728 | tf_op jit(solution)/shard_map/all_to_all | solution.py:56
  438.2 10.6 %all-gather.5.cloned.1.call-done = bf16[16,48,2048]{2,1,0:T(8,128)(2,1)} async-done(((bf16[16,48,1024]{2,1,0:T(8,128)(2,1)}), bf16[16,48,2048]{2,1,0:T(8,128)(2,1)}) %all-gather.5.cloned.1.call-update) | async-done | bytes 3145744 | tf_op jit(solution)/shard_map/all_gather | solution.py:59
  448.7 7.3 %gather_fusion.1 = bf16[384,2048]{1,0:T(8,128)(2,1)} fusion(bf16[768,2048]{1,0:T(8,128)(2,1)} %bitcast.43, s32[1024]{0:T(1024)S(1)} %pad_clamp_fusion), kind=kCustom, calls=%fused_computation.1 | custom fusion | bytes 3147264 | tf_op jit(solution)/shard_map/gather | solution.py:60
  456.1 3.4 reshape.184
  466.4 4.6 copy.36
  471.0 4.6 copy.37
  (39 shorter events, 17.8 us)
Async XLA Ops:
  22.2 11.1 %copy-start.2 = (f32[128]{0:T(128)S(1)}, f32[128]{0:T(128)}, u32[]{:S(2)}) copy-start(f32[128]{0:T(128)} %param.10) | copy-start | bytes 1540
  24.9 42.6 %all-to-all-start = ((bf16[16,48,1024]{2,1,0:T(8,128)(2,1)}), bf16[16,48,1024]{2,1,0:T(8,128)(2,1)}, u32[]{:S(2)}, u32[]{:S(2)}) async-start(bf16[16,48,1024]{2,1,0:T(8,128)(2,1)} %constant_dynamic-slice_fusion), calls=%async_computation | async-start | bytes 3145728 | tf_op jit(solution)/shard_map/all_to_all | solution.py:45
  173.1 83.0 %all-to-all-start.2 = ((bf16[16,128,1024]{2,1,0:T(8,128)(2,1)}), bf16[16,128,1024]{2,1,0:T(8,128)(2,1)}, u32[]{:S(2)}, u32[]{:S(2)}) async-start(bf16[16,128,1024]{2,1,0:T(8,128)(2,1)} %bitcast.47), calls=%async_computation.2 | async-start | bytes 8388608 | tf_op jit(solution)/shard_map/all_to_all | solution.py:22
  258.7 97.0 %all-to-all-start.3 = ((bf16[16,128,1024]{2,1,0:T(8,128)(2,1)}), bf16[16,128,1024]{2,1,0:T(8,128)(2,1)}, u32[]{:S(2)}, u32[]{:S(2)}) async-start(bf16[16,128,1024]{2,1,0:T(8,128)(2,1)} %bitcast.46), calls=%async_computation.3 | async-start | bytes 8388608 | tf_op jit(solution)/shard_map/all_to_all | solution.py:23
  277.3 15.7 %all-gather.3.cloned.1.call-start = ((), (), s32[]{:S(2)}) async-start(), calls=%async_computation.6 | async-start | bytes 4718592 | tf_op jit(solution)/shard_map/all_gather | solution.py:48
  278.0 115.2 %reduce-scatter.2.cloned.1.call-start = ((), (), s32[]{:S(2)}) async-start(), calls=%async_computation.7 | async-start | bytes 4718592 | tf_op jit(solution)/shard_map/reduce_scatter | solution.py:53
  368.3 69.8 %copy-start.1 = (f32[192,2]{0,1:T(2,128)S(1)}, f32[192,2]{0,1:T(2,128)}, u32[]{:S(2)}) copy-start(f32[192,2]{0,1:T(2,128)} %param.9) | copy-start | bytes 4612
  368.3 80.4 %all-gather.5.cloned.1.call-start = ((), (), s32[]{:S(2)}) async-start(), calls=%async_computation.8 | async-start | bytes 4718592 | tf_op jit(solution)/shard_map/all_gather | solution.py:59
  459.5 4.9 %copy-start = (bf16[16,128,1024]{2,1,0:T(8,128)(2,1)S(1)}, bf16[16,128,1024]{2,1,0:T(8,128)(2,1)}, u32[]{:S(2)}) copy-start(bf16[16,128,1024]{2,1,0:T(8,128)(2,1)} %all_to_all.46) | copy-start | bytes 12582916
Sparse Core Ops, SparseCore 0:
  279.6 13.3 all-gather.2
  368.4 24.7 reduce-scatter.1
  438.2 10.4 all-gather.4
where the time goes:
time: 483 us; the launch traced here: 482 us
  waiting for transfers between devices  209 us (43%)
  blocking collectives  146 us (30%)
  local copies, waits for them, and re-layouts  43.4 us (9%)
  starting transfers between devices  31.8 us (7%)
  matrix products  20.8 us (4%)
  other arithmetic  17.3 us (4%)
  between operations  13.9 us (3%)
    all_to_all x1, blocking collectives, body(): lax.all_to_all(gate_send, 'fs', split_axis=0, concat_axis=1, tiled=True)  101 us
    all_to_all x1, waiting for transfers between devices, body(): lax.all_to_all(up_send, 'fs', split_axis=0, concat_axis=1, tiled=True)  75.9 us
    all_to_all x1, waiting for transfers between devices, body(): lax.all_to_all(down_send, 'fs', split_axis=0, concat_axis=1, tiled=True)  54.5 us
    all_to_all x1, blocking collectives, body(): lax.all_to_all(share.reshape(fs_count, per_peer, col_count), 'fs', split_...  44.9 us
    all_to_all x1, waiting for transfers between devices, body(): lax.all_to_all(own_cols, 'fs', split_axis=0, concat_axis=0, tiled=True)  28 us
    reduce_scatter x1, waiting for transfers between devices, body(): lax.psum_scatter(partial_value.astype(jnp.bfloat16), 'tp', scatter_dimens...  24.9 us
    all_to_all x1, starting transfers between devices, body(): lax.all_to_all(down_send, 'fs', split_axis=0, concat_axis=1, tiled=True)  18.6 us
    all_gather x1, waiting for transfers between devices, body(): piece = lax.all_gather(arrived, 'tp', axis=1, tiled=True)  14.8 us
  transfers between devices with their start and end apart: 6, of which 6 were waited for; matrix products, arithmetic and copies ran while one was open for 3% of the time, Pallas kernels for 0%

commit v1 on v0

--- a/solution.py
+++ b/solution.py
@@ -19,7 +19,10 @@
     down_send = jnp.repeat(down_weight.astype(jnp.bfloat16), copies, axis=0)
     gate_new, up_new, down_new = (
         lax.all_to_all(gate_send, "fs", split_axis=0, concat_axis=1, tiled=True),
-        lax.all_to_all(up_send, "fs", split_axis=0, concat_axis=1, tiled=True),
+        jnp.concatenate(
+            lax.all_to_all(jnp.stack(jnp.split(up_send, lax.axis_size("fs"), axis=0)), "fs", 0, 0),
+            axis=1,
+        ),
         lax.all_to_all(down_send, "fs", split_axis=0, concat_axis=1, tiled=True),
     )
     values = tokens.astype(jnp.float32)

time: 483 us -> 481 us (level)
  local copies, waits for them, and re-layouts: 43.4 us -> 53.5 us
  waiting for transfers between devices: 209 us -> 199 us
    unnamed x10 -> x25, local copies, waits for them, and re-layouts: 12.1 us -> 23.1 us
    all_to_all x1, waiting for transfers between devices: 28 us -> 17.3 us  [body(): lax.all_to_all(own_cols, 'fs', split_axis=0, concat_axis=0, tiled=True)]
  transfers between devices with their start and end apart: 6 -> 6, of which waited for: 6 -> 6; matrix products, arithmetic and copies ran while one was open for 3% -> 6% of each run, Pallas kernels for 0% -> 0%
where the time goes in v1:
time: 481 us; the launch traced here: 480 us
  waiting for transfers between devices  199 us (41%)
  blocking collectives  146 us (30%)
  local copies, waits for them, and re-layouts  53.5 us (11%)
  starting transfers between devices  31.8 us (7%)
  matrix products  20.7 us (4%)
  other arithmetic  15.9 us (3%)
  between operations  13.9 us (3%)
    all_to_all x1, blocking collectives, body(): lax.all_to_all(jnp.stack(jnp.split(up_send, lax.axis_size('fs'), axis=0))...  101 us
    all_to_all x1, waiting for transfers between devices, body(): lax.all_to_all(gate_send, 'fs', split_axis=0, concat_axis=1, tiled=True)  75.9 us
    all_to_all x1, waiting for transfers between devices, body(): lax.all_to_all(down_send, 'fs', split_axis=0, concat_axis=1, tiled=True)  54.5 us
    all_to_all x1, blocking collectives, body(): lax.all_to_all(share.reshape(fs_count, per_peer, col_count), 'fs', split_...  44.9 us
    reduce_scatter x1, waiting for transfers between devices, body(): lax.psum_scatter(partial_value.astype(jnp.bfloat16), 'tp', scatter_dimens...  24.9 us
    unnamed x25, local copies, waits for them, and re-layouts  23.1 us
    all_to_all x1, starting transfers between devices, body(): lax.all_to_all(down_send, 'fs', split_axis=0, concat_axis=1, tiled=True)  18.5 us
    all_to_all x1, waiting for transfers between devices, body(): lax.all_to_all(own_cols, 'fs', split_axis=0, concat_axis=0, tiled=True)  17.3 us
  transfers between devices with their start and end apart: 6, of which 6 were waited for; matrix products, arithmetic and copies ran while one was open for 6% of the time, Pallas kernels for 0%

profile of v1, /device:TPU:0, one launch (start us, length us, event | category | flops | bytes accessed | tf_op | source)
XLA Modules:
  0.0 480.4 jit_solution(3566671061701294676)
XLA Ops:
  10.5 2.9 scatter_custom_fusion
  18.0 4.2 gather_fusion
  22.2 2.7 constant_dynamic-slice_fusion
  24.9 8.4 %all-to-all-start = ((bf16[16,48,1024]{2,1,0:T(8,128)(2,1)}), bf16[16,48,1024]{2,1,0:T(8,128)(2,1)}, u32[]{:S(2)}, u32[]{:S(2)}) async-start(bf16[16,48,1024]{2,1,0:T(8,128)(2,1)} %constant_dynamic-slice_fusion), calls=%async_computation | async-start | bytes 3145728 | tf_op jit(solution)/shard_map/all_to_all | solution.py:48
  33.3 4.8 multiply_convert_fusion
  50.2 17.3 %all-to-all-done = bf16[16,48,1024]{2,1,0:T(8,128)(2,1)} async-done(((bf16[16,48,1024]{2,1,0:T(8,128)(2,1)}), bf16[16,48,1024]{2,1,0:T(8,128)(2,1)}, u32[]{:S(2)}, u32[]{:S(2)}) %all-to-all-start) | async-done | bytes 1572896 | tf_op jit(solution)/shard_map/all_to_all | solution.py:48
  67.5 101.1 %all_to_all.39 = bf16[16,1,128,1024]{3,2,1,0:T(8,128)(2,1)} all-to-all(bf16[16,1,128,1024]{3,2,1,0:T(8,128)(2,1)} %fusion.8), channel_id=1, replica_groups=mesh['fs'=16,'tp'=2] {'fs'}, dimensions={0} | all-to-all | bytes 8388608 | tf_op jit(solution)/shard_map/all_to_all | solution.py:23
  168.5 2.6 broadcast_in_dim.12
  171.2 4.6 all-to-all-start.1
  175.7 2.5 convert_element_type.44
  178.3 75.9 %all-to-all-done.1 = bf16[16,128,1024]{2,1,0:T(8,128)(2,1)} async-done(((bf16[16,128,1024]{2,1,0:T(8,128)(2,1)}), bf16[16,128,1024]{2,1,0:T(8,128)(2,1)}, u32[]{:S(2)}, u32[]{:S(2)}) %all-to-all-start.1) | async-done | bytes 4194336 | tf_op jit(solution)/shard_map/all_to_all | solution.py:21
  254.2 2.6 broadcast_in_dim.28
  256.8 18.5 %all-to-all-start.3 = ((bf16[16,128,1024]{2,1,0:T(8,128)(2,1)}), bf16[16,128,1024]{2,1,0:T(8,128)(2,1)}, u32[]{:S(2)}, u32[]{:S(2)}) async-start(bf16[16,128,1024]{2,1,0:T(8,128)(2,1)} %bitcast.126), calls=%async_computation.3 | async-start | bytes 8388608 | tf_op jit(solution)/shard_map/all_to_all | solution.py:26
  276.3 14.8 %all-gather.3.cloned.1.call-done = bf16[768,2048]{1,0:T(8,128)(2,1)} async-done(((bf16[768,1024]{1,0:T(8,128)(2,1)}), bf16[768,2048]{1,0:T(8,128)(2,1)}) %all-gather.3.cloned.1.call-update) | async-done | bytes 3145744 | tf_op jit(solution)/shard_map/all_gather | solution.py:51
  291.1 8.2 %fusion.36 = f32[768,1024]{1,0:T(8,128)} fusion(bf16[768,2048]{1,0:T(8,128)(2,1)} %all-gather.3.cloned.1.call-done, bf16[2048,1024]{1,0:T(8,128)(2,1)} %bitcast.6), kind=kOutput, calls=%fused_computation.86 | convolution fusion | flops 3221225472 | bytes 10485760 | tf_op jit(solution)/shard_map/dot_general | solution.py:52
  299.3 54.5 %all-to-all-done.3 = bf16[16,128,1024]{2,1,0:T(8,128)(2,1)} async-done(((bf16[16,128,1024]{2,1,0:T(8,128)(2,1)}), bf16[16,128,1024]{2,1,0:T(8,128)(2,1)}, u32[]{:S(2)}, u32[]{:S(2)}) %all-to-all-start.3) | async-done | bytes 4194336 | tf_op jit(solution)/shard_map/all_to_all | solution.py:26
  353.8 12.5 %convolution_convert_fusion = bf16[768,2048]{1,0:T(8,128)(2,1)} fusion(bf16[2048,1024]{1,0:T(8,128)(2,1)} %bitcast.26, f32[768,1024]{1,0:T(8,128)} %fusion.36, bf16[768,2048]{1,0:T(8,128)(2,1)} %all-gather.3.cloned.1.call-done, bf16[2048,1024]{1,0:T(8,128)(2,1)} %bitcast.124), kind=kOutput, calls=%fused_computation.5 | convolution fusion | flops 6448742400 | bytes 17825792 | tf_op jit(solution)/shard_map/rf,df->rd/dot_general | solution.py:55
  366.4 24.9 %reduce-scatter.2.cloned.1.call-done = bf16[768,1024]{1,0:T(8,128)(2,1)} async-done(((bf16[768,2048]{1,0:T(8,128)(2,1)}), bf16[768,1024]{1,0:T(8,128)(2,1)}) %reduce-scatter.2.cloned.1.call-update) | async-done | bytes 1572880 | tf_op jit(solution)/shard_map/reduce_scatter | solution.py:56
  391.3 44.9 %all_to_all.40 = bf16[16,48,1024]{2,1,0:T(8,128)(2,1)} all-to-all(bf16[16,48,1024]{2,1,0:T(8,128)(2,1)} %bitcast.129), channel_id=1, replica_groups=mesh['fs'=16,'tp'=2] {'fs'}, dimensions={0} | all-to-all | bytes 3145728 | tf_op jit(solution)/shard_map/all_to_all | solution.py:59
  436.2 10.6 %all-gather.5.cloned.1.call-done = bf16[16,48,2048]{2,1,0:T(8,128)(2,1)} async-done(((bf16[16,48,1024]{2,1,0:T(8,128)(2,1)}), bf16[16,48,2048]{2,1,0:T(8,128)(2,1)}) %all-gather.5.cloned.1.call-update) | async-done | bytes 3145744 | tf_op jit(solution)/shard_map/all_gather | solution.py:62
  446.8 7.3 %gather_fusion.1 = bf16[384,2048]{1,0:T(8,128)(2,1)} fusion(bf16[768,2048]{1,0:T(8,128)(2,1)} %bitcast.107, s32[1024]{0:T(1024)S(1)} %pad_clamp_fusion), kind=kCustom, calls=%fused_computation.1 | custom fusion | bytes 3147264 | tf_op jit(solution)/shard_map/gather | solution.py:63
  454.1 3.4 reshape.183
  462.4 4.8 %copy.85 = bf16[1,2048,1024]{2,1,0:T(8,128)(2,1)} copy(bf16[1,2048,1024]{2,1,0:T(8,128)(2,1)} %bitcast.32) | data formatting | bytes 8388608
  469.3 4.6 copy.87
  (55 shorter events, 27.8 us)
Async XLA Ops:
  22.2 11.1 %copy-start.2 = (f32[128]{0:T(128)S(1)}, f32[128]{0:T(128)}, u32[]{:S(2)}) copy-start(f32[128]{0:T(128)} %param.10) | copy-start | bytes 1540
  24.9 42.6 %all-to-all-start = ((bf16[16,48,1024]{2,1,0:T(8,128)(2,1)}), bf16[16,48,1024]{2,1,0:T(8,128)(2,1)}, u32[]{:S(2)}, u32[]{:S(2)}) async-start(bf16[16,48,1024]{2,1,0:T(8,128)(2,1)} %constant_dynamic-slice_fusion), calls=%async_computation | async-start | bytes 3145728 | tf_op jit(solution)/shard_map/all_to_all | solution.py:48
  171.2 83.0 %all-to-all-start.1 = ((bf16[16,128,1024]{2,1,0:T(8,128)(2,1)}), bf16[16,128,1024]{2,1,0:T(8,128)(2,1)}, u32[]{:S(2)}, u32[]{:S(2)}) async-start(bf16[16,128,1024]{2,1,0:T(8,128)(2,1)} %bitcast.127), calls=%async_computation.1 | async-start | bytes 8388608 | tf_op jit(solution)/shard_map/all_to_all | solution.py:21
  256.8 97.0 %all-to-all-start.3 = ((bf16[16,128,1024]{2,1,0:T(8,128)(2,1)}), bf16[16,128,1024]{2,1,0:T(8,128)(2,1)}, u32[]{:S(2)}, u32[]{:S(2)}) async-start(bf16[16,128,1024]{2,1,0:T(8,128)(2,1)} %bitcast.126), calls=%async_computation.3 | async-start | bytes 8388608 | tf_op jit(solution)/shard_map/all_to_all | solution.py:26
  275.3 15.7 %all-gather.3.cloned.1.call-start = ((), (), s32[]{:S(2)}) async-start(), calls=%async_computation.6 | async-start | bytes 4718592 | tf_op jit(solution)/shard_map/all_gather | solution.py:51
  276.1 115.2 %reduce-scatter.2.cloned.1.call-start = ((), (), s32[]{:S(2)}) async-start(), calls=%async_computation.7 | async-start | bytes 4718592 | tf_op jit(solution)/shard_map/reduce_scatter | solution.py:56
  366.3 69.9 %copy-start.1 = (f32[192,2]{0,1:T(2,128)S(1)}, f32[192,2]{0,1:T(2,128)}, u32[]{:S(2)}) copy-start(f32[192,2]{0,1:T(2,128)} %param.9) | copy-start | bytes 4612
  366.3 80.4 %all-gather.5.cloned.1.call-start = ((), (), s32[]{:S(2)}) async-start(), calls=%async_computation.8 | async-start | bytes 4718592 | tf_op jit(solution)/shard_map/all_gather | solution.py:62
  462.4 4.8 %copy-start = (bf16[16,1,128,1024]{3,2,1,0:T(8,128)(2,1)S(1)}, bf16[16,1,128,1024]{3,2,1,0:T(8,128)(2,1)}, u32[]{:S(2)}) copy-start(bf16[16,1,128,1024]{3,2,1,0:T(8,128)(2,1)} %all_to_all.39) | copy-start | bytes 12582916
Sparse Core Ops, SparseCore 0:
  277.7 13.3 all-gather.2
  366.5 24.7 reduce-scatter.1
  436.3 10.4 all-gather.4
